TPU v7x, 32 devices: a whole 2x2x4 slice. The times are simulated.
32 devices in a mesh: sp: 8 (over z, y), tp: 4 (over x, core).
Axes of the slice: x: 2, y: 2, z: 4, core: 2. Of those that a mesh axis runs over, the one named last changes fastest.
Arguments:
- hidden: bfloat16 [6144, 2048], P(('sp', 'tp')), may hold values from -6 to 6
- norm_gain: float32 [2, 2048], replicated, may hold values from 0.1 to 1.9
- w_value: bfloat16 [2, 2048, 2048], P(None, 'sp', 'tp'), may hold values from -0.125 to 0.125
- w_gate: bfloat16 [2, 2048, 2048], P(None, 'sp', 'tp'), may hold values from -0.125 to 0.125
- conv_weight: float32 [2, 31, 2048], P(None, None, 'tp'), may hold values from -3 to 3
- conv_bias: float32 [2, 2048], P(None, 'tp'), may hold values from -3 to 3
- chan_gain: float32 [2, 2048], P(None, 'tp'), may hold values from 0.1 to 1.9
- chan_shift: float32 [2, 2048], P(None, 'tp'), may hold values from -3 to 3
- w_out: bfloat16 [2, 2048, 2048], P(None, 'tp', 'sp'), may hold values from -0.125 to 0.125
Outputs:
- result: bfloat16 [6144, 2048], P(('sp', 'tp'))
All inputs are finite; a program needn't handle non-finite values.
Results may differ from a plain program's by a relative error of at most 0.015.
Values may be sent and summed in bfloat16 or wider, within the bound.
A program may use at most 64 MiB of HBM per device.

v0:
```python
import jax
import jax.numpy as jnp
from jax import lax
from jax.sharding import PartitionSpec as P

EPS = 1e-06


def shifted(shard, axis, by):
    size = lax.axis_size(axis)
    pairs = [(i, i + by) for i in range(size) if 0 <= i + by < size]
    return lax.ppermute(shard, axis, pairs)


def body(hidden, norm_gain, w_value, w_gate, conv_weight, conv_bias, chan_gain, chan_shift, w_out):
    group = lax.axis_size("tp")
    own_rows = hidden.shape[0]
    chans = w_value.shape[2]
    taps = conv_weight.shape[1]
    state = hidden
    for layer in range(norm_gain.shape[0]):
        xf = state.astype(jnp.float32)
        scale = lax.rsqrt(jnp.mean(xf * xf, axis=1, keepdims=True) + EPS)
        normed = (xf * scale * norm_gain[layer][None, :]).astype(jnp.bfloat16)
        tokens = lax.all_gather(normed, "tp", axis=0, tiled=True)
        empty = jnp.zeros((tokens.shape[0], chans), jnp.float32)

        def add_both(totals, pieces, start, tokens=tokens):
            return (
                jnp.dot(tokens, pieces[0], preferred_element_type=jnp.float32),
                jnp.dot(tokens, pieces[1], preferred_element_type=jnp.float32),
            )

        lin, gate = add_both(
            (empty, empty),
            (
                lax.all_gather(w_value[layer], "sp", axis=0, tiled=True),
                lax.all_gather(w_gate[layer], "sp", axis=0, tiled=True),
            ),
            jnp.int32(0),
        )
        glu = (lin * jax.nn.sigmoid(gate)).astype(jnp.bfloat16)
        before = shifted(glu[tokens.shape[0] - (taps - 1) :], "sp", 1)
        window = jnp.concatenate([before, glu], axis=0).astype(jnp.float32)
        length = tokens.shape[0]
        mixed = jnp.zeros((length, chans), jnp.float32) + conv_bias[layer][None, :]
        for tap in range(taps):
            mixed = mixed + conv_weight[layer, tap][None, :] * window[tap : tap + length]
        totals = lax.psum((jnp.sum(mixed, axis=1), jnp.sum(mixed * mixed, axis=1)), "tp")
        mean = (totals[0] / (chans * group))[:, None]
        msq = (totals[1] / (chans * group))[:, None]
        var = msq - mean * mean
        act = jax.nn.silu(
            (mixed - mean) * lax.rsqrt(var + EPS) * chan_gain[layer][None, :]
            + chan_shift[layer][None, :]
        ).astype(jnp.bfloat16)

        def project(piece, start, act=act):
            return jnp.dot(act, piece, preferred_element_type=jnp.float32)

        partial_out = project(lax.all_gather(w_out[layer], "sp", axis=1, tiled=True), jnp.int32(0))

        def take_rows(start, count, partial_out=partial_out):
            return partial_out

        update = lax.psum_scatter(
            take_rows(jnp.int32(0), own_rows * lax.axis_size("tp")).astype(jnp.bfloat16),
            "tp",
            scatter_dimension=0,
            tiled=True,
        ).astype(jnp.float32)
        state = (xf + update).astype(jnp.bfloat16)
    return state


def solution(mesh):
    placed = (
        P(("sp", "tp"), None),
        P(),
        P(None, "sp", "tp"),
        P(None, "sp", "tp"),
        P(None, None, "tp"),
        P(None, "tp"),
        P(None, "tp"),
        P(None, "tp"),
        P(None, "tp", "sp"),
    )
    return jax.shard_map(
        body, mesh=mesh, in_specs=placed, out_specs=P(("sp", "tp"), None), check_vma=False
    )
```

profile of v0, /device:TPU:0, one launch (start us, length us, event | category | flops | bytes accessed | tf_op | source)
XLA Modules:
  0.0 466.3 jit_solution(699687578448124518)
XLA Ops:
  6.5 2.0 fusion.101
  12.1 49.2 %all-gather.21.cloned.1.call-done = bf16[1,2048,512]{2,1,0:T(8,128)(2,1)} async-done(((bf16[1,256,512]{2,1,0:T(8,128)(2,1)}), bf16[1,2048,512]{2,1,0:T(8,128)(2,1)}) %all-gather.21.cloned.1.call-update) | async-done | bytes 2097168 | tf_op jit(solution)/shard_map/all_gather | solution.py:38
  61.3 28.6 %all-gather.15.cloned.1.call-done = bf16[768,2048]{1,0:T(8,128)(2,1)} async-done(((bf16[192,2048]{1,0:T(8,128)(2,1)}), bf16[768,2048]{1,0:T(8,128)(2,1)}) %all-gather.15.cloned.1.call-update) | async-done | bytes 3145744 | tf_op jit(solution)/shard_map/all_gather | solution.py:25
  89.9 4.3 fusion.6
  94.3 46.9 %all-gather.19.cloned.1.call-done = bf16[1,2048,512]{2,1,0:T(8,128)(2,1)} async-done(((bf16[1,256,512]{2,1,0:T(8,128)(2,1)}), bf16[1,2048,512]{2,1,0:T(8,128)(2,1)}) %all-gather.19.cloned.1.call-update) | async-done | bytes 2097168 | tf_op jit(solution)/shard_map/all_gather | solution.py:37
  141.2 4.5 multiply_convert_fusion.3
  145.7 2.5 collective-permute-start
  150.0 6.9 %fusion.97 = (f32[768]{0:T(1024)S(1)}, f32[768]{0:T(1024)S(1)}, f32[768,512]{1,0:T(8,128)S(1)}) fusion(f32[798,512]{1,0:T(8,128)S(1)} %maximum_convert_fusion, f32[512]{0:T(512)S(1)} %bitcast.128, f32[512]{0:T(512)S(1)} %bitcast.129, f32[512]{0:T(512)S(1)} %bitcast.130, f32[512]{0:T(512)S(1)} %bitcast.131, f32[512]{0:T(512)S(1)} %bitcast.132, ...), kind=kLoop, calls=%fused_computation.177 | loop fusion | flops 25557504 | bytes 50403328 | tf_op jit(solution)/shard_map/reduce_sum | solution.py:49
  156.9 6.2 %all-reduce.1 = (f32[768]{0:T(1024)S(1)}, f32[768]{0:T(1024)S(1)}) all-reduce(f32[768]{0:T(1024)S(1)} %get-tuple-element.8, f32[768]{0:T(1024)S(1)} %get-tuple-element.7), channel_id=1, replica_groups=mesh['sp'=8,'tp'=4] {'tp'}, use_global_device_ids=true, to_apply=%region_4.0 | all-reduce | flops 1536 | bytes 12288 | tf_op jit(solution)/shard_map/psum | solution.py:49
  163.1 28.9 %all-gather.23.cloned.1.call-done = bf16[1,512,2048]{2,1,0:T(8,128)(2,1)} async-done(((bf16[1,512,256]{2,1,0:T(8,128)(2,1)}), bf16[1,512,2048]{2,1,0:T(8,128)(2,1)}) %all-gather.23.cloned.1.call-update) | async-done | bytes 2097168 | tf_op jit(solution)/shard_map/all_gather | solution.py:61
  192.0 5.3 %convolution_convert_fusion.1 = bf16[768,2048]{1,0:T(8,128)(2,1)} fusion(bf16[1,512,2048]{2,1,0:T(8,128)(2,1)} %all-gather.23.cloned.1.call-done, f32[768,512]{1,0:T(8,128)S(1)} %get-tuple-element.14, f32[512]{0:T(512)S(1)} %bitcast.165, f32[512]{0:T(512)S(1)} %bitcast.164, f32[768]{0:T(1024)S(1)} %get-tuple-element.94, f32[768]{0:T(1024)S(1)} %get-tuple-element.93), kind=kOutput, calls=%fused_computation.1 | convolution fusion | flops 1615724544 | bytes 6825984 | tf_op jit(solution)/shard_map/dot_general | solution.py:59
  198.0 35.6 %reduce-scatter.3.cloned.1.call-done = bf16[192,2048]{1,0:T(8,128)(2,1)} async-done(((bf16[768,2048]{1,0:T(8,128)(2,1)}), bf16[192,2048]{1,0:T(8,128)(2,1)}) %reduce-scatter.3.cloned.1.call-update) | async-done | bytes 786448 | tf_op jit(solution)/shard_map/reduce_scatter | solution.py:66
  237.9 46.8 %all-gather.27.cloned.1.call-done = bf16[1,2048,512]{2,1,0:T(8,128)(2,1)} async-done(((bf16[1,256,512]{2,1,0:T(8,128)(2,1)}), bf16[1,2048,512]{2,1,0:T(8,128)(2,1)}) %all-gather.27.cloned.1.call-update) | async-done | bytes 2097168 | tf_op jit(solution)/shard_map/all_gather | solution.py:38
  284.7 28.6 %all-gather.17.cloned.1.call-done = bf16[768,2048]{1,0:T(8,128)(2,1)} async-done(((bf16[192,2048]{1,0:T(8,128)(2,1)}), bf16[768,2048]{1,0:T(8,128)(2,1)}) %all-gather.17.cloned.1.call-update) | async-done | bytes 3145744 | tf_op jit(solution)/shard_map/all_gather | solution.py:25
  313.3 4.3 fusion.1
  317.6 46.9 %all-gather.25.cloned.1.call-done = bf16[1,2048,512]{2,1,0:T(8,128)(2,1)} async-done(((bf16[1,256,512]{2,1,0:T(8,128)(2,1)}), bf16[1,2048,512]{2,1,0:T(8,128)(2,1)}) %all-gather.25.cloned.1.call-update) | async-done | bytes 2097168 | tf_op jit(solution)/shard_map/all_gather | solution.py:37
  364.5 4.5 multiply_convert_fusion.1
  369.0 2.7 collective-permute-start.1
  373.3 6.9 %fusion.96 = (f32[768]{0:T(1024)S(1)}, f32[768]{0:T(1024)S(1)}, f32[768,512]{1,0:T(8,128)S(1)}) fusion(f32[798,512]{1,0:T(8,128)S(1)} %maximum_convert_fusion.1, f32[512]{0:T(512)S(1)} %bitcast.109, f32[512]{0:T(512)S(1)} %bitcast.98, f32[512]{0:T(512)S(1)} %bitcast.142, f32[512]{0:T(512)S(1)} %bitcast.143, f32[512]{0:T(512)S(1)} %bitcast.144, ...), kind=kLoop, calls=%fused_computation.176 | loop fusion | flops 25557504 | bytes 50403328 | tf_op jit(solution)/shard_map/reduce_sum | solution.py:49
  380.2 6.2 %all-reduce = (f32[768]{0:T(1024)S(1)}, f32[768]{0:T(1024)S(1)}) all-reduce(f32[768]{0:T(1024)S(1)} %get-tuple-element.6, f32[768]{0:T(1024)S(1)} %get-tuple-element.5), channel_id=1, replica_groups=mesh['sp'=8,'tp'=4] {'tp'}, use_global_device_ids=true, to_apply=%region_10.11 | all-reduce | flops 1536 | bytes 12288 | tf_op jit(solution)/shard_map/psum | solution.py:49
  386.4 29.1 %all-gather.29.cloned.1.call-done = bf16[1,512,2048]{2,1,0:T(8,128)(2,1)} async-done(((bf16[1,512,256]{2,1,0:T(8,128)(2,1)}), bf16[1,512,2048]{2,1,0:T(8,128)(2,1)}) %all-gather.29.cloned.1.call-update) | async-done | bytes 2097168 | tf_op jit(solution)/shard_map/all_gather | solution.py:61
  415.5 5.3 %convolution_convert_fusion = bf16[768,2048]{1,0:T(8,128)(2,1)} fusion(bf16[1,512,2048]{2,1,0:T(8,128)(2,1)} %all-gather.29.cloned.1.call-done, f32[768,512]{1,0:T(8,128)S(1)} %get-tuple-element.13, f32[512]{0:T(512)S(1)} %bitcast.163, f32[512]{0:T(512)S(1)} %bitcast.162, f32[768]{0:T(1024)S(1)} %get-tuple-element.86, f32[768]{0:T(1024)S(1)} %get-tuple-element.85), kind=kOutput, calls=%fused_computation | convolution fusion | flops 1615724544 | bytes 6825984 | tf_op jit(solution)/shard_map/dot_general | solution.py:59
  420.9 36.2 %reduce-scatter.5.cloned.1.call-done = bf16[192,2048]{1,0:T(8,128)(2,1)} async-done(((bf16[768,2048]{1,0:T(8,128)(2,1)}), bf16[192,2048]{1,0:T(8,128)(2,1)}) %reduce-scatter.5.cloned.1.call-update) | async-done | bytes 786448 | tf_op jit(solution)/shard_map/reduce_scatter | solution.py:66
  457.1 2.4 fusion.17
  (62 shorter events, 11.8 us)
Async XLA Ops:
  6.5 2.1 copy-start
  6.5 2.3 copy-start.5
  6.5 54.8 %all-gather.21.cloned.1.call-start = ((), (), s32[]{:S(2)}) async-start(), calls=%async_computation.7 | async-start | bytes 2359296 | tf_op jit(solution)/shard_map/all_gather | solution.py:38
  8.5 1.6 copy-start.2
  8.5 81.4 %all-gather.15.cloned.1.call-start = ((), (), s32[]{:S(2)}) async-start(), calls=%async_computation.2 | async-start | bytes 3932160 | tf_op jit(solution)/shard_map/all_gather | solution.py:25
  8.9 2.2 copy-start.3
  10.0 2.0 copy-start.4
  10.0 2.0 copy-start.6
  10.1 2.1 copy-start.7
  10.1 131.1 %all-gather.19.cloned.1.call-start = ((), (), s32[]{:S(2)}) async-start(), calls=%async_computation.6 | async-start | bytes 2359296 | tf_op jit(solution)/shard_map/all_gather | solution.py:37
  11.0 181.0 %all-gather.23.cloned.1.call-start = ((), (), s32[]{:S(2)}) async-start(), calls=%async_computation.8 | async-start | bytes 2359296 | tf_op jit(solution)/shard_map/all_gather | solution.py:61
  11.9 221.6 %reduce-scatter.3.cloned.1.call-start = ((), (), s32[]{:S(2)}) async-start(), calls=%async_computation.3 | async-start | bytes 3932160 | tf_op jit(solution)/shard_map/reduce_scatter | solution.py:66
  94.3 53.9 %copy-start.8 = (f32[2,512]{1,0:T(2,128)S(1)}, f32[2,512]{1,0:T(2,128)}, u32[]{:S(2)}) copy-start(f32[2,512]{1,0:T(2,128)} %param.16) | copy-start | bytes 12292
  145.7 4.0 collective-permute-start
  197.4 87.3 %all-gather.27.cloned.1.call-start = ((), (), s32[]{:S(2)}) async-start(), calls=%async_computation.10 | async-start | bytes 2359296 | tf_op jit(solution)/shard_map/all_gather | solution.py:38
  197.9 115.4 %all-gather.17.cloned.1.call-start = ((), (), s32[]{:S(2)}) async-start(), calls=%async_computation.4 | async-start | bytes 3932160 | tf_op jit(solution)/shard_map/all_gather | solution.py:25
  233.5 1.6 copy-start.1
  236.4 128.2 %all-gather.25.cloned.1.call-start = ((), (), s32[]{:S(2)}) async-start(), calls=%async_computation.9 | async-start | bytes 2359296 | tf_op jit(solution)/shard_map/all_gather | solution.py:37
  237.1 178.4 %all-gather.29.cloned.1.call-start = ((), (), s32[]{:S(2)}) async-start(), calls=%async_computation.11 | async-start | bytes 2359296 | tf_op jit(solution)/shard_map/all_gather | solution.py:61
  237.8 219.2 %reduce-scatter.5.cloned.1.call-start = ((), (), s32[]{:S(2)}) async-start(), calls=%async_computation.5 | async-start | bytes 3932160 | tf_op jit(solution)/shard_map/reduce_scatter | solution.py:66
  369.0 4.1 collective-permute-start.1
Sparse Core Ops, SparseCore 0:
  9.5 51.7 all-gather.20
  62.9 27.0 all-gather.14
  92.1 49.0 all-gather.18
  143.1 48.8 all-gather.22
  197.5 36.0 reduce-scatter.2
  235.5 49.0 all-gather.26
  286.2 27.0 all-gather.16
  315.4 49.0 all-gather.24
  366.6 48.8 all-gather.28
  421.0 36.0 reduce-scatter.4
where the time goes:
time: 467 us; the launch traced here: 466 us
  waiting for transfers between devices  382 us (82%)
  matrix products  28.3 us (6%)
  other arithmetic  20.8 us (4%)
  between operations  13.8 us (3%)
  blocking collectives  12.3 us (3%)
  starting transfers between devices  5.48 us (1%)
    all_gather x2, waiting for transfers between devices, body(): lax.all_gather(w_gate[layer], 'sp', axis=0, tiled=True)  95.9 us
    all_gather x2, waiting for transfers between devices, body(): lax.all_gather(w_value[layer], 'sp', axis=0, tiled=True)  93.8 us
    reduce_scatter x2, waiting for transfers between devices, body(): lax.psum_scatter(take_rows(jnp.int32(0), own_rows * lax.axis_size('tp'))....  71.8 us
    all_gather x2, waiting for transfers between devices, body(): lax.all_gather(w_out[layer], 'sp', axis=1, tiled=True)  58 us
    all_gather x2, waiting for transfers between devices, body(): tokens = lax.all_gather(normed, 'tp', axis=0, tiled=True)  57.3 us
    reduce_sum x2, other arithmetic, body(): jnp.sum(mixed, axis=1)  13.8 us
    psum x2, blocking collectives, body(): lax.psum((jnp.sum(mixed, axis=1), jnp.sum(mixed * mixed, axis=1)), 'tp')  12.3 us
    dot_general x2, matrix products, project(): return jnp.dot(act, piece, preferred_element_type=jnp.float32)  10.7 us
  transfers between devices with their start and end apart: 12, of which 12 were waited for; matrix products, arithmetic and copies ran while one was open for 8% of the time, Pallas kernels for 0%

commit v1 on v0

--- a/solution.py
+++ b/solution.py
@@ -58,7 +58,9 @@
         def project(piece, start, act=act):
             return jnp.dot(act, piece, preferred_element_type=jnp.float32)
 
-        partial_out = project(lax.all_gather(w_out[layer], "sp", axis=1, tiled=True), jnp.int32(0))
+        partial_out = project(
+            jnp.concatenate(lax.all_gather(w_out[layer], "sp"), axis=1), jnp.int32(0)
+        )
 
         def take_rows(start, count, partial_out=partial_out):
             return partial_out

time: 467 us -> 500 us (1.071)
  waiting for transfers between devices: 382 us -> 405 us
  local copies, waits for them, and re-layouts: 3.88 us -> 11.5 us
    all_gather x2, waiting for transfers between devices: 58 us -> 84 us  [body(): lax.all_gather(w_out[layer], 'sp')]
    all_gather x0 -> x2, local copies, waits for them, and re-layouts: none -> 6.78 us  [body(): lax.all_gather(w_out[layer], 'sp')]
  transfers between devices with their start and end apart: 12 -> 12, of which waited for: 12 -> 10; matrix products, arithmetic and copies ran while one was open for 8% -> 6% of each run, Pallas kernels for 0% -> 0%
where the time goes in v1:
time: 500 us; the launch traced here: 499 us
  waiting for transfers between devices  405 us (81%)
  matrix products  29.6 us (6%)
  other arithmetic  22.6 us (5%)
  between operations  13.8 us (3%)
  local copies, waits for them, and re-layouts  11.5 us (2%)
  blocking collectives  11.5 us (2%)
  starting transfers between devices  5.47 us (1%)
    all_gather x2, waiting for transfers between devices, body(): lax.all_gather(w_gate[layer], 'sp', axis=0, tiled=True)  96 us
    all_gather x2, waiting for transfers between devices, body(): lax.all_gather(w_value[layer], 'sp', axis=0, tiled=True)  92.7 us
    all_gather x2, waiting for transfers between devices, body(): lax.all_gather(w_out[layer], 'sp')  84 us
    reduce_scatter x2, waiting for transfers between devices, body(): lax.psum_scatter(take_rows(jnp.int32(0), own_rows * lax.axis_size('tp'))....  73.1 us
    all_gather x2, waiting for transfers between devices, body(): tokens = lax.all_gather(normed, 'tp', axis=0, tiled=True)  57.3 us
    reduce_sum x2, other arithmetic, body(): jnp.sum(mixed, axis=1)  14.4 us
    psum x2, blocking collectives, body(): lax.psum((jnp.sum(mixed, axis=1), jnp.sum(mixed * mixed, axis=1)), 'tp')  11.5 us
    dot_general x2, matrix products, project(): return jnp.dot(act, piece, preferred_element_type=jnp.float32)  10.4 us
  transfers between devices with their start and end apart: 12, of which 10 were waited for; matrix products, arithmetic and copies ran while one was open for 6% of the time, Pallas kernels for 0%

profile of v1, /device:TPU:0, one launch (start us, length us, event | category | flops | bytes accessed | tf_op | source)
XLA Modules:
  0.0 499.5 jit_solution(4980373221902320031)
XLA Ops:
  12.1 49.2 %all-gather.23.cloned.1.call-done = bf16[1,2048,512]{2,1,0:T(8,128)(2,1)} async-done(((bf16[1,256,512]{2,1,0:T(8,128)(2,1)}), bf16[1,2048,512]{2,1,0:T(8,128)(2,1)}) %all-gather.23.cloned.1.call-update) | async-done | bytes 2097168 | tf_op jit(solution)/shard_map/all_gather | solution.py:38
  61.3 28.6 %all-gather.13.cloned.1.call-done = bf16[768,2048]{1,0:T(8,128)(2,1)} async-done(((bf16[192,2048]{1,0:T(8,128)(2,1)}), bf16[768,2048]{1,0:T(8,128)(2,1)}) %all-gather.13.cloned.1.call-update) | async-done | bytes 3145744 | tf_op jit(solution)/shard_map/all_gather | solution.py:25
  89.9 4.3 fusion.4
  94.3 46.9 %all-gather.21.cloned.1.call-done = bf16[1,2048,512]{2,1,0:T(8,128)(2,1)} async-done(((bf16[1,256,512]{2,1,0:T(8,128)(2,1)}), bf16[1,2048,512]{2,1,0:T(8,128)(2,1)}) %all-gather.21.cloned.1.call-update) | async-done | bytes 2097168 | tf_op jit(solution)/shard_map/all_gather | solution.py:37
  141.2 4.5 multiply_convert_fusion.3
  146.5 2.5 collective-permute-start
  149.0 41.8 %all-gather.15.cloned.1.call-done = bf16[8,512,256]{2,1,0:T(8,128)(2,1)} async-done(((bf16[1,512,256]{2,1,0:T(8,128)(2,1)}), bf16[8,512,256]{2,1,0:T(8,128)(2,1)}) %all-gather.15.cloned.1.call-update) | async-done | bytes 2097168 | tf_op jit(solution)/shard_map/all_gather | solution.py:62
  190.8 2.9 copy.12
  195.1 7.5 %fusion.95 = (f32[768]{0:T(1024)S(1)}, f32[768]{0:T(1024)S(1)}, f32[768,512]{1,0:T(8,128)}) fusion(f32[798,512]{1,0:T(8,128)S(1)} %maximum_convert_fusion, f32[512]{0:T(512)S(1)} %bitcast.136, f32[512]{0:T(512)S(1)} %bitcast.137, f32[512]{0:T(512)S(1)} %bitcast.138, f32[512]{0:T(512)S(1)} %bitcast.139, f32[512]{0:T(512)S(1)} %bitcast.140, ...), kind=kLoop, calls=%fused_computation.175 | loop fusion | flops 25557504 | bytes 50403328 | tf_op jit(solution)/shard_map/reduce_sum | solution.py:49
  202.6 5.7 %all-reduce.1 = (f32[768]{0:T(1024)S(1)}, f32[768]{0:T(1024)S(1)}) all-reduce(f32[768]{0:T(1024)S(1)} %get-tuple-element.8, f32[768]{0:T(1024)S(1)} %get-tuple-element.7), channel_id=1, replica_groups=mesh['sp'=8,'tp'=4] {'tp'}, use_global_device_ids=true, to_apply=%region_4.0 | all-reduce | flops 1536 | bytes 12288 | tf_op jit(solution)/shard_map/psum | solution.py:49
  208.3 5.1 %convolution_convert_fusion.1 = bf16[768,2048]{1,0:T(8,128)(2,1)} fusion(bf16[512,2048]{0,1:T(8,128)(2,1)S(1)} %bitcast.99, f32[768,512]{1,0:T(8,128)} %get-tuple-element.14, f32[512]{0:T(512)S(1)} %bitcast.169, f32[512]{0:T(512)S(1)} %bitcast.168, f32[768]{0:T(1024)S(1)} %get-tuple-element.94, f32[768]{0:T(1024)S(1)} %get-tuple-element.93), kind=kOutput, calls=%fused_computation.1 | convolution fusion | flops 1615724544 | bytes 6825984 | tf_op jit(solution)/shard_map/dot_general | solution.py:59
  214.1 36.2 %reduce-scatter.3.cloned.1.call-done = bf16[192,2048]{1,0:T(8,128)(2,1)} async-done(((bf16[768,2048]{1,0:T(8,128)(2,1)}), bf16[192,2048]{1,0:T(8,128)(2,1)}) %reduce-scatter.3.cloned.1.call-update) | async-done | bytes 786448 | tf_op jit(solution)/shard_map/reduce_scatter | solution.py:68
  254.7 46.8 %all-gather.27.cloned.1.call-done = bf16[1,2048,512]{2,1,0:T(8,128)(2,1)} async-done(((bf16[1,256,512]{2,1,0:T(8,128)(2,1)}), bf16[1,2048,512]{2,1,0:T(8,128)(2,1)}) %all-gather.27.cloned.1.call-update) | async-done | bytes 2097168 | tf_op jit(solution)/shard_map/all_gather | solution.py:38
  301.4 28.6 %all-gather.17.cloned.1.call-done = bf16[768,2048]{1,0:T(8,128)(2,1)} async-done(((bf16[192,2048]{1,0:T(8,128)(2,1)}), bf16[768,2048]{1,0:T(8,128)(2,1)}) %all-gather.17.cloned.1.call-update) | async-done | bytes 3145744 | tf_op jit(solution)/shard_map/all_gather | solution.py:25
  330.1 5.5 %fusion = f32[768,512]{1,0:T(8,128)} fusion(bf16[768,2048]{1,0:T(8,128)(2,1)} %all-gather.17.cloned.1.call-done, bf16[1,2048,512]{2,1,0:T(8,128)(2,1)} %all-gather.27.cloned.1.call-done), kind=kOutput, calls=%fused_computation.8 | convolution fusion | flops 1610612736 | bytes 6815744 | tf_op jit(solution)/shard_map/dot_general | solution.py:31
  335.5 45.8 %all-gather.25.cloned.1.call-done = bf16[1,2048,512]{2,1,0:T(8,128)(2,1)} async-done(((bf16[1,256,512]{2,1,0:T(8,128)(2,1)}), bf16[1,2048,512]{2,1,0:T(8,128)(2,1)}) %all-gather.25.cloned.1.call-update) | async-done | bytes 2097168 | tf_op jit(solution)/shard_map/all_gather | solution.py:37
  381.3 4.9 multiply_convert_fusion.1
  386.2 2.6 collective-permute-start.1
  388.9 42.2 %all-gather.19.cloned.1.call-done = bf16[8,512,256]{2,1,0:T(8,128)(2,1)} async-done(((bf16[1,512,256]{2,1,0:T(8,128)(2,1)}), bf16[8,512,256]{2,1,0:T(8,128)(2,1)}) %all-gather.19.cloned.1.call-update) | async-done | bytes 2097168 | tf_op jit(solution)/shard_map/all_gather | solution.py:62
  431.2 3.9 copy.13
  435.3 6.9 %fusion.94 = (f32[768]{0:T(1024)S(1)}, f32[768]{0:T(1024)S(1)}, f32[768,512]{1,0:T(8,128)S(1)}) fusion(f32[798,512]{1,0:T(8,128)S(1)} %maximum_convert_fusion.1, f32[512]{0:T(512)S(1)} %bitcast.102, f32[512]{0:T(512)S(1)} %bitcast.103, f32[512]{0:T(512)S(1)} %bitcast.146, f32[512]{0:T(512)S(1)} %bitcast.147, f32[512]{0:T(512)S(1)} %bitcast.148, ...), kind=kLoop, calls=%fused_computation.174 | loop fusion | flops 25557504 | bytes 50403328 | tf_op jit(solution)/shard_map/reduce_sum | solution.py:49
  442.2 5.8 %all-reduce = (f32[768]{0:T(1024)S(1)}, f32[768]{0:T(1024)S(1)}) all-reduce(f32[768]{0:T(1024)S(1)} %get-tuple-element.6, f32[768]{0:T(1024)S(1)} %get-tuple-element.5), channel_id=1, replica_groups=mesh['sp'=8,'tp'=4] {'tp'}, use_global_device_ids=true, to_apply=%region_10.11 | all-reduce | flops 1536 | bytes 12288 | tf_op jit(solution)/shard_map/psum | solution.py:49
  448.0 5.3 %convolution_convert_fusion = bf16[768,2048]{1,0:T(8,128)(2,1)} fusion(bf16[512,2048]{0,1:T(8,128)(2,1)} %bitcast.98, f32[768,512]{1,0:T(8,128)S(1)} %get-tuple-element.13, f32[512]{0:T(512)S(1)} %bitcast.167, f32[512]{0:T(512)S(1)} %bitcast.166, f32[768]{0:T(1024)S(1)} %get-tuple-element.86, f32[768]{0:T(1024)S(1)} %get-tuple-element.85), kind=kOutput, calls=%fused_computation | convolution fusion | flops 1615724544 | bytes 6825984 | tf_op jit(solution)/shard_map/dot_general | solution.py:59
  453.4 36.9 %reduce-scatter.5.cloned.1.call-done = bf16[192,2048]{1,0:T(8,128)(2,1)} async-done(((bf16[768,2048]{1,0:T(8,128)(2,1)}), bf16[192,2048]{1,0:T(8,128)(2,1)}) %reduce-scatter.5.cloned.1.call-update) | async-done | bytes 786448 | tf_op jit(solution)/shard_map/reduce_scatter | solution.py:68
  (66 shorter events, 15.3 us)
Async XLA Ops:
  6.5 2.0 copy-start
  6.5 2.3 copy-start.6
  6.5 54.8 %all-gather.23.cloned.1.call-start = ((), (), s32[]{:S(2)}) async-start(), calls=%async_computation.9 | async-start | bytes 2359296 | tf_op jit(solution)/shard_map/all_gather | solution.py:38
  8.5 1.6 copy-start.3
  8.5 81.4 %all-gather.13.cloned.1.call-start = ((), (), s32[]{:S(2)}) async-start(), calls=%async_computation.2 | async-start | bytes 3932160 | tf_op jit(solution)/shard_map/all_gather | solution.py:25
  8.8 2.1 copy-start.4
  10.0 1.9 copy-start.7
  10.0 1.9 copy-start.8
  10.0 2.0 copy-start.5
  10.0 131.2 %all-gather.21.cloned.1.call-start = ((), (), s32[]{:S(2)}) async-start(), calls=%async_computation.8 | async-start | bytes 2359296 | tf_op jit(solution)/shard_map/all_gather | solution.py:37
  10.9 179.9 %all-gather.15.cloned.1.call-start = ((), (), s32[]{:S(2)}) async-start(), calls=%async_computation.3 | async-start | bytes 2359296 | tf_op jit(solution)/shard_map/all_gather | solution.py:62
  11.8 238.5 %reduce-scatter.3.cloned.1.call-start = ((), (), s32[]{:S(2)}) async-start(), calls=%async_computation.4 | async-start | bytes 3932160 | tf_op jit(solution)/shard_map/reduce_scatter | solution.py:68
  94.3 54.8 %copy-start.9 = (f32[2,512]{1,0:T(2,128)S(1)}, f32[2,512]{1,0:T(2,128)}, u32[]{:S(2)}) copy-start(f32[2,512]{1,0:T(2,128)} %param.16) | copy-start | bytes 12292
  145.6 0.9 copy-start.2
  146.5 47.1 %collective-permute-start = (bf16[30,512]{1,0:T(8,128)(2,1)S(1)}, bf16[30,512]{1,0:T(8,128)(2,1)S(1)}, u32[]{:S(2)}, u32[]{:S(2)}) collective-permute-start(bf16[30,512]{1,0:T(8,128)(2,1)S(1)} %slice.560), channel_id=1, source_target_pairs={{0,4},{4,8},{8,12},{12,16},{16,20},{20,24},{24,28},{1,5},{5,9},{9,... | collective-permute-start | bytes 92168 | tf_op jit(solution)/shard_map/ppermute | solution.py:12
  213.5 88.0 %all-gather.27.cloned.1.call-start = ((), (), s32[]{:S(2)}) async-start(), calls=%async_computation.11 | async-start | bytes 2359296 | tf_op jit(solution)/shard_map/all_gather | solution.py:38
  214.1 116.0 %all-gather.17.cloned.1.call-start = ((), (), s32[]{:S(2)}) async-start(), calls=%async_computation.5 | async-start | bytes 3932160 | tf_op jit(solution)/shard_map/all_gather | solution.py:25
  250.3 1.6 copy-start.1
  253.2 128.2 %all-gather.25.cloned.1.call-start = ((), (), s32[]{:S(2)}) async-start(), calls=%async_computation.10 | async-start | bytes 2359296 | tf_op jit(solution)/shard_map/all_gather | solution.py:37
  253.9 177.3 %all-gather.19.cloned.1.call-start = ((), (), s32[]{:S(2)}) async-start(), calls=%async_computation.6 | async-start | bytes 2359296 | tf_op jit(solution)/shard_map/all_gather | solution.py:62
  254.6 235.6 %reduce-scatter.5.cloned.1.call-start = ((), (), s32[]{:S(2)}) async-start(), calls=%async_computation.7 | async-start | bytes 3932160 | tf_op jit(solution)/shard_map/reduce_scatter | solution.py:68
  386.2 48.9 %collective-permute-start.1 = (bf16[30,512]{1,0:T(8,128)(2,1)S(1)}, bf16[30,512]{1,0:T(8,128)(2,1)S(1)}, u32[]{:S(2)}, u32[]{:S(2)}) collective-permute-start(bf16[30,512]{1,0:T(8,128)(2,1)S(1)} %slice.592), channel_id=1, source_target_pairs={{0,4},{4,8},{8,12},{12,16},{16,20},{20,24},{24,28},{1,5},{5,9},{9,... | collective-permute-start | bytes 92168 | tf_op jit(solution)/shard_map/ppermute | solution.py:12
Sparse Core Ops, SparseCore 0:
  9.5 51.7 all-gather.22
  62.9 27.0 all-gather.12
  92.1 49.0 all-gather.20
  143.2 47.5 all-gather.14
  213.6 36.6 reduce-scatter.2
  252.3 49.0 all-gather.26
  303.0 27.0 all-gather.16
  332.2 49.0 all-gather.24
  383.4 47.6 all-gather.18
  453.5 36.6 reduce-scatter.4
